TPU v7x, 32 devices: a whole 2x2x4 slice. The times are simulated.
32 devices in a mesh: rep: 2 (over x), fs: 8 (over z, y), tp: 2 (over core).
Axes of the slice: x: 2, y: 2, z: 4, core: 2. Of those that a mesh axis runs over, the one named last changes fastest.
Arguments:
- tokens: bfloat16 [6144, 2048], P(('rep', 'fs', 'tp')), may hold values from -6 to 6
- mix_gain_in: float32 [2048], replicated, may hold values from 0.1 to 1.9
- pool_weight: bfloat16 [4, 512, 512], P(None, 'fs'), may hold values from -0.25 to 0.25
- mix_gain_out: float32 [2048], replicated, may hold values from 0.1 to 1.9
- ffn_gain_in: float32 [2048], replicated, may hold values from 0.1 to 1.9
- gate_weight: bfloat16 [2048, 5632], P('fs', 'tp'), may hold values from -0.125 to 0.125
- up_weight: bfloat16 [2048, 5632], P('fs', 'tp'), may hold values from -0.125 to 0.125
- gate_taps: float32 [3, 5632], replicated, may hold values from -3.5 to 3.5
- up_taps: float32 [3, 5632], replicated, may hold values from -3.5 to 3.5
- down_weight: bfloat16 [5632, 2048], P('tp', 'fs'), may hold values from -0.078125 to 0.078125
- ffn_gain_out: float32 [2048], replicated, may hold values from 0.1 to 1.9
Outputs:
- mixed_out: bfloat16 [6144, 2048], P(('rep', 'fs', 'tp'))
All inputs are finite; a program needn't handle non-finite values.
Results may differ from a plain program's by a relative error of at most 0.014.
Values may be sent and summed in bfloat16 or wider, within the bound.
A program may use at most 128 MiB of HBM per device.

v0:
```python
import jax
import jax.numpy as jnp
from jax import lax
from jax.sharding import PartitionSpec as P

pool_spans = (2, 4, 8, 16)
rms_eps = 1e-06


def rms_scale(values, gain):
    floats = values.astype(jnp.float32)
    return floats * lax.rsqrt(jnp.mean(floats * floats, axis=-1, keepdims=True) + rms_eps) * gain


def pooled_gap(padded, count):
    margin = padded.shape[0] - count
    floats = padded.astype(jnp.float32)
    width = padded.shape[1] // len(pool_spans)
    where = jnp.arange(count, dtype=jnp.int32)
    pieces = []
    for group, span in enumerate(pool_spans):
        block = floats[:, group * width : (group + 1) * width]
        total = jnp.zeros((count, width), jnp.float32)
        for back in range(span):
            total = total + block[margin - back : margin - back + count]
        divisor = jnp.minimum(where + 1, span).astype(jnp.float32)
        pieces.append(total / divisor[:, None] - block[margin:])
    return jnp.concatenate(pieces, axis=1).astype(jnp.bfloat16)


def mix_groups(gap, pool_full):
    length, features = gap.shape
    groups = pool_full.shape[0]
    shaped = gap.reshape(length, groups, features // groups)
    result = jnp.einsum("rgc,gcj->rgj", shaped, pool_full, preferred_element_type=jnp.float32)
    return result.reshape(length, features).astype(jnp.bfloat16)


def causal_taps(pre, taps):
    width = taps.shape[0]
    floats = pre.astype(jnp.float32)
    padded = jnp.concatenate([jnp.zeros((width - 1, pre.shape[1]), jnp.float32), floats], axis=0)
    total = jnp.zeros(floats.shape, jnp.float32)
    for offset in range(width):
        total = total + taps[offset] * padded[offset : offset + pre.shape[0]]
    return total


def shards(
    tokens,
    mix_gain_in,
    pool_weight,
    mix_gain_out,
    ffn_gain_in,
    gate_weight,
    up_weight,
    gate_taps,
    up_taps,
    down_weight,
    ffn_gain_out,
):
    rows, features = tokens.shape
    margin = max(pool_spans) - 1
    position = lax.axis_index("tp")
    pool_full = lax.all_gather(pool_weight, "fs", axis=1, tiled=True)
    every = lax.all_gather(tokens, "tp", axis=0, tiled=True)
    length = every.shape[0]
    normed = rms_scale(every, mix_gain_in).astype(jnp.bfloat16)
    padded = jnp.concatenate([jnp.zeros((margin, features), jnp.bfloat16), normed], axis=0)
    gap = pooled_gap(padded, length)
    mixed = mix_groups(gap, pool_full)
    after_all = every.astype(jnp.float32) + rms_scale(mixed, mix_gain_out)
    whole = rms_scale(after_all, ffn_gain_in).astype(jnp.bfloat16)
    after_mix = lax.dynamic_slice_in_dim(after_all, position * rows, rows, 0)
    columns = gate_weight.shape[1]
    gate_part = jnp.dot(
        whole,
        lax.all_gather(gate_weight, "fs", axis=0, tiled=True),
        preferred_element_type=jnp.float32,
    )
    up_part = jnp.dot(
        whole,
        lax.all_gather(up_weight, "fs", axis=0, tiled=True),
        preferred_element_type=jnp.float32,
    )
    offset = position * columns
    gate_local = lax.dynamic_slice_in_dim(gate_taps, offset, columns, 1)
    up_local = lax.dynamic_slice_in_dim(up_taps, offset, columns, 1)
    gate_conv = causal_taps(gate_part.astype(jnp.bfloat16), gate_local)
    up_conv = causal_taps(up_part.astype(jnp.bfloat16), up_local)
    hidden = (jax.nn.gelu(gate_conv, approximate=True) * up_conv).astype(jnp.bfloat16)
    down_full = lax.all_gather(down_weight, "fs", axis=1, tiled=True)
    channel_out = lax.psum_scatter(
        jnp.dot(hidden, down_full, preferred_element_type=jnp.float32).astype(jnp.bfloat16),
        "tp",
        scatter_dimension=0,
        tiled=True,
    ).astype(jnp.float32)
    return (after_mix + rms_scale(channel_out, ffn_gain_out)).astype(jnp.bfloat16)


def solution(mesh):
    in_specs = (
        P(("rep", "fs", "tp"), None),
        P(),
        P(None, "fs", None),
        P(),
        P(),
        P("fs", "tp"),
        P("fs", "tp"),
        P(),
        P(),
        P("tp", "fs"),
        P(),
    )
    out_specs = P(("rep", "fs", "tp"), None)
    return jax.shard_map(shards, mesh=mesh, in_specs=in_specs, out_specs=out_specs, check_vma=False)
```

profile of v0, /device:TPU:0, one launch (start us, length us, event | category | flops | bytes accessed | tf_op | source)
XLA Modules:
  0.0 600.9 jit_solution(8342491924516857888)
XLA Ops:
  6.5 0.7 all-gather.6.cloned.1.call-update
  7.3 0.0 all-gather.8.cloned.1.call-start
  7.3 0.7 all-gather.8.cloned.1.call-update
  8.0 0.0 all-gather.10.cloned.1.call-start
  8.1 0.7 all-gather.10.cloned.1.call-update
  8.8 0.0 all-gather.12.cloned.1.call-start
  8.8 0.5 all-gather.12.cloned.1.call-update
  9.3 0.0 all-gather.14.cloned.1.call-start
  9.4 0.5 all-gather.14.cloned.1.call-update
  9.9 0.0 reduce-scatter.2.cloned.1.call-start
  10.0 1.2 dynamic-slice_reduce_fusion.2
  11.2 10.2 %all-gather.6.cloned.1.call-done = bf16[384,2048]{1,0:T(8,128)(2,1)} async-done(((bf16[192,2048]{1,0:T(8,128)(2,1)}), bf16[384,2048]{1,0:T(8,128)(2,1)}) %all-gather.6.cloned.1.call-update) | async-done | bytes 1572880 | tf_op jit(solution)/shard_map/all_gather | solution.py:66
  21.4 1.8 fusion.12
  23.2 1.8 fusion.14
  25.1 0.5 pad_convert_fusion
  25.5 1.0 fusion.51
  26.5 1.2 fusion.48
  27.7 46.2 %all-gather.8.cloned.1.call-done = bf16[4,512,512]{2,1,0:T(8,128)(2,1)} async-done(((bf16[4,64,512]{2,1,0:T(8,128)(2,1)}), bf16[4,512,512]{2,1,0:T(8,128)(2,1)}) %all-gather.8.cloned.1.call-update) | async-done | bytes 2097168 | tf_op jit(solution)/shard_map/all_gather | solution.py:65
  73.9 2.7 fusion.11
  76.6 0.4 convert_bitcast_fusion
  77.0 0.3 copy.13
  77.3 1.1 copy-done
  78.4 0.8 multiply_reduce_fusion
  79.2 158.8 %all-gather.10.cloned.1.call-done = bf16[2048,2816]{1,0:T(8,128)(2,1)} async-done(((bf16[256,2816]{1,0:T(8,128)(2,1)}), bf16[2048,2816]{1,0:T(8,128)(2,1)}) %all-gather.10.cloned.1.call-update) | async-done | bytes 11534352 | tf_op jit(solution)/shard_map/all_gather | solution.py:78
  238.0 9.7 %fusion.10 = f32[384,2816]{1,0:T(8,128)} fusion(bf16[2048,2816]{1,0:T(8,128)(2,1)} %all-gather.10.cloned.1.call-done, f32[384,2048]{1,0:T(8,128)S(1)} %get-tuple-element.12, f32[2048]{0:T(1024)S(1)} %copy-done.4, f32[384]{0:T(512)S(1)} %add_rsqrt_fusion), kind=kOutput, calls=%fused_computation.16 | convolution fusion | flops 4433707008 | bytes 19015168 | tf_op jit(solution)/shard_map/dot_general | solution.py:76
  247.6 153.9 %all-gather.12.cloned.1.call-done = bf16[2048,2816]{1,0:T(8,128)(2,1)} async-done(((bf16[256,2816]{1,0:T(8,128)(2,1)}), bf16[2048,2816]{1,0:T(8,128)(2,1)}) %all-gather.12.cloned.1.call-update) | async-done | bytes 11534352 | tf_op jit(solution)/shard_map/all_gather | solution.py:83
  401.5 9.6 %fusion.9 = f32[384,2816]{1,0:T(8,128)} fusion(bf16[2048,2816]{1,0:T(8,128)(2,1)} %all-gather.12.cloned.1.call-done, f32[384,2048]{1,0:T(8,128)S(1)} %get-tuple-element.12, f32[2048]{0:T(1024)S(1)} %copy-done.4, f32[384]{0:T(512)S(1)} %add_rsqrt_fusion), kind=kOutput, calls=%fused_computation.14 | convolution fusion | flops 4433707008 | bytes 19015168 | tf_op jit(solution)/shard_map/dot_general | solution.py:81
  411.1 153.8 %all-gather.14.cloned.1.call-done = bf16[2816,2048]{1,0:T(8,128)(2,1)} async-done(((bf16[2816,256]{1,0:T(8,128)(2,1)}), bf16[2816,2048]{1,0:T(8,128)(2,1)}) %all-gather.14.cloned.1.call-update) | async-done | bytes 11534352 | tf_op jit(solution)/shard_map/all_gather | solution.py:92
  565.0 18.0 %convolution_convert_fusion.2 = bf16[384,2048]{1,0:T(8,128)(2,1)} fusion(bf16[2816,2048]{1,0:T(8,128)(2,1)} %all-gather.14.cloned.1.call-done, f32[384,2816]{1,0:T(8,128)} %fusion.9, f32[384,2816]{1,0:T(8,128)} %fusion.10, f32[2816]{0:T(1024)S(1)} %get-tuple-element.10, f32[2816]{0:T(1024)S(1)} %get-tuple-element.9, f32[2816]{0:T(1024)S(1)} %get-tuple-element.8, ...), kind=kOutput, calls=%fused_computation.25 | convolution fusion | flops 4451598336 | bytes 21825536 | tf_op jit(solution)/shard_map/dot_general | solution.py:94
  583.0 7.4 %reduce-scatter.2.cloned.1.call-done = bf16[192,2048]{1,0:T(8,128)(2,1)} async-done(((bf16[384,2048]{1,0:T(8,128)(2,1)}), bf16[192,2048]{1,0:T(8,128)(2,1)}) %reduce-scatter.2.cloned.1.call-update) | async-done | bytes 786448 | tf_op jit(solution)/shard_map/reduce_scatter | solution.py:93
  590.3 1.4 fusion.25
  591.7 2.3 fusion.28
  (18 shorter events, 0.1 us)
Async XLA Ops:
  6.5 14.9 %all-gather.6.cloned.1.call-start = ((), (), s32[]{:S(2)}) async-start(), calls=%async_computation.1 | async-start | bytes 2359296 | tf_op jit(solution)/shard_map/all_gather | solution.py:66
  7.3 16.0 %copy-start.1 = (f32[2048]{0:T(1024)S(1)}, f32[2048]{0:T(1024)}, u32[]{:S(2)}) copy-start(f32[2048]{0:T(1024)} %param.12) | copy-start | bytes 24580
  7.3 66.6 %all-gather.8.cloned.1.call-start = ((), (), s32[]{:S(2)}) async-start(), calls=%async_computation.2 | async-start | bytes 2359296 | tf_op jit(solution)/shard_map/all_gather | solution.py:65
  8.0 229.9 %all-gather.10.cloned.1.call-start = ((), (), s32[]{:S(2)}) async-start(), calls=%async_computation.3 | async-start | bytes 12976128 | tf_op jit(solution)/shard_map/all_gather | solution.py:78
  8.8 392.8 %all-gather.12.cloned.1.call-start = ((), (), s32[]{:S(2)}) async-start(), calls=%async_computation.4 | async-start | bytes 12976128 | tf_op jit(solution)/shard_map/all_gather | solution.py:83
  9.3 555.6 %all-gather.14.cloned.1.call-start = ((), (), s32[]{:S(2)}) async-start(), calls=%async_computation.5 | async-start | bytes 12976128 | tf_op jit(solution)/shard_map/all_gather | solution.py:92
  9.9 580.4 %reduce-scatter.2.cloned.1.call-start = ((), (), s32[]{:S(2)}) async-start(), calls=%async_computation.6 | async-start | bytes 2359296 | tf_op jit(solution)/shard_map/reduce_scatter | solution.py:93
  77.0 1.4 copy-start
  77.0 1.4 copy-start.3
  78.4 159.6 %copy-start.4 = (f32[2048]{0:T(1024)S(1)}, f32[2048]{0:T(1024)}, u32[]{:S(2)}) copy-start(f32[2048]{0:T(1024)} %param.15) | copy-start | bytes 24580
  565.0 26.8 %copy-start.2 = (f32[2048]{0:T(1024)S(1)}, f32[2048]{0:T(1024)}, u32[]{:S(2)}) copy-start(f32[2048]{0:T(1024)} %param.21) | copy-start | bytes 24580
Sparse Core Ops, SparseCore 0:
  8.9 12.5 all-gather.5
  23.6 50.2 all-gather.7
  76.1 161.8 all-gather.9
  240.0 161.4 all-gather.11
  403.4 161.4 all-gather.13
  583.1 7.2 reduce-scatter.1
where the time goes:
time: 601 us
  waiting for transfers between devices  533 us (89%)
  matrix products  39.9 us (7%)
  between operations  13.6 us (2%)
  other arithmetic  11.2 us (2%)
    all_gather x1, waiting for transfers between devices, shards(): lax.all_gather(gate_weight, 'fs', axis=0, tiled=True)  159 us
    all_gather x1, waiting for transfers between devices, shards(): lax.all_gather(up_weight, 'fs', axis=0, tiled=True)  154 us
    all_gather x1, waiting for transfers between devices, shards(): down_full = lax.all_gather(down_weight, 'fs', axis=1, tiled=True)  154 us
    all_gather x1, waiting for transfers between devices, shards(): pool_full = lax.all_gather(pool_weight, 'fs', axis=1, tiled=True)  46.2 us
    dot_general x1, matrix products, shards(): jnp.dot(hidden, down_full, preferred_element_type=jnp.float32)  18 us
  transfers between devices with their start and end apart: 6, of which 6 were waited for; matrix products, arithmetic and copies ran while one was open for 5% of the time, Pallas kernels for 0%

commit v1 on v0

v1 whole, which is shorter than its diff:
```python
import functools

import jax
import jax.numpy as jnp
from jax import lax
from jax.experimental import pallas as pl
from jax.experimental.pallas import tpu as pltpu
from jax.sharding import PartitionSpec as P

MESH = pl.DeviceIdType.MESH
pool_spans = (2, 4, 8, 16)
rms_eps = 1e-06
weight_budget = 24 * 2**20
f32 = jnp.float32
bf16 = jnp.bfloat16


def rms_scale(floats, gain):
    return floats * lax.rsqrt(jnp.mean(floats * floats, axis=-1, keepdims=True) + rms_eps) * gain


def gelu(v):
    return 0.5 * v * (1.0 + jnp.tanh(0.7978845608028654 * (v + 0.044715 * v * v * v)))


class Plan:
    def __init__(self, mesh, depth, width, columns):
        self.R, self.F, self.T = mesh.shape["rep"], mesh.shape["fs"], mesh.shape["tp"]
        self.Y = 1
        while 4 * self.Y * self.Y <= self.F:
            self.Y *= 2
        while self.F % self.Y:
            self.Y -= 1
        self.Z = self.F // self.Y
        self.joined = 3 * width * columns * 2 > weight_budget
        self.n_sub = self.R * self.Y if self.joined else 1
        self.G = self.T * self.n_sub
        self.cols = columns // self.n_sub


def kernel(
    plan, tokens, gain_in, pool, gain_out, gain_ffn, w, gate_taps, up_taps, gain_last, out,
    halo, pool_all, w_gu, w_d, x_all, normed, after, acc_g, acc_u, hidden, partial, got,
    own_sem, halo_sem, y_ss, up_ss, dn_ss, piece_rs, share_ss, share_rs, x_ss, x_rs, p_ss, p_rs,
):
    R, F, T, Y, Z, G, cols = plan.R, plan.F, plan.T, plan.Y, plan.Z, plan.G, plan.cols
    r, f, t = lax.axis_index("rep"), lax.axis_index("fs"), lax.axis_index("tp")
    z, y = f // Y, f % Y
    rows, width = tokens.shape
    depth = width // F
    groups, gc = pool_all.shape[0], pool_all.shape[1]
    slab = gc // F
    S = min(T, groups)
    GS = groups // S
    q = t % S
    margin = halo.shape[0]
    POOL, GU, DN = 0, 1, 2

    if plan.joined:
        me = (r * Y + y) * T + t
    else:
        me = t

    def member(g):
        if plan.joined:
            return {"rep": g // (T * Y), "fs": z * Y + (g // T) % Y, "tp": g % T}
        return {"tp": g}

    def sub_of(y_to):
        return r * Y + y_to if plan.joined else 0

    def w_rows(y_to):
        return pl.ds(pl.multiple_of(sub_of(y_to) * cols, 64 if cols % 64 == 0 else 8), cols)

    def slot(kind, origin):
        if kind == POOL:
            return pool_all.at[pl.ds(q * GS, GS), pl.ds(pl.multiple_of(origin * slab, slab), slab)]
        return w_gu.at[origin] if kind == GU else w_d.at[origin]

    def source(kind, y_to):
        if kind == POOL:
            return pool.at[pl.ds(q * GS, GS)]
        if kind == GU:
            return w.at[pl.ds(0, 2), w_rows(y_to)]
        return w.at[2, w_rows(y_to)]

    def own_copy(kind):
        return pltpu.make_async_copy(source(kind, y), slot(kind, f), own_sem.at[kind])

    def y_copy(kind, step):
        y_to = (y + step) % Y
        return pltpu.make_async_remote_copy(
            src_ref=source(kind, y_to), dst_ref=slot(kind, f), send_sem=y_ss.at[kind, step - 1],
            recv_sem=piece_rs.at[kind, f], device_id={"fs": z * Y + y_to}, device_id_type=MESH)

    def chain_copy(kind, origin, dz):
        return pltpu.make_async_remote_copy(
            src_ref=slot(kind, origin), dst_ref=slot(kind, origin), send_sem=(up_ss if dz > 0 else dn_ss).at[kind, origin],
            recv_sem=piece_rs.at[kind, origin], device_id={"fs": (z + dz) * Y + y}, device_id_type=MESH)

    def send_up(kind, origin):
        @pl.when(z + 1 < Z)
        def _():
            chain_copy(kind, origin, 1).start()

    def send_down(kind, origin):
        @pl.when(z > 0)
        def _():
            chain_copy(kind, origin, -1).start()

    def arrived(kind, origin):
        chain_copy(kind, origin, 1).wait_recv()

    def chain_plane(kind):
        own_copy(kind).wait()
        send_up(kind, f)
        send_down(kind, f)
        for step in range(1, Y):
            origin = z * Y + (y + step) % Y
            arrived(kind, origin)
            send_up(kind, origin)
            send_down(kind, origin)

    def chain_step(kind, s, use=None):
        for step in range(Y):
            @pl.when(z >= s)
            def _():
                origin = (z - s) * Y + (y + step) % Y
                arrived(kind, origin)
                send_up(kind, origin)

            @pl.when(z + s < Z)
            def _():
                origin = (z + s) * Y + (y + step) % Y
                arrived(kind, origin)
                send_down(kind, origin)
        if use is not None:
            use_step(s, use)

    def use_step(s, use):
        for sign in (-1, 1):
            @pl.when((z >= s) if sign < 0 else (z + s < Z))
            def _():
                def body(step, carry):
                    use((z + sign * s) * Y + (y + step) % Y)
                    return carry
                lax.fori_loop(0, Y, body, 0)

    def use_plane(use):
        def body(step, carry):
            use(z * Y + (y + step) % Y)
            return carry
        lax.fori_loop(0, Y, body, 0)

    def halo_copy():
        return pltpu.make_async_remote_copy(
            src_ref=tokens.at[pl.ds(rows - margin, margin)], dst_ref=halo, send_sem=halo_sem.at[0],
            recv_sem=halo_sem.at[1], device_id={"tp": (t + 1) % T}, device_id_type=MESH)

    def share_copy(step, q_from):
        return pltpu.make_async_remote_copy(
            src_ref=pool_all.at[pl.ds(q_from * GS, GS)], dst_ref=pool_all.at[pl.ds(q_from * GS, GS)],
            send_sem=share_ss.at[step - 1], recv_sem=share_rs.at[q_from],
            device_id={"tp": t - q + (q + step) % S}, device_id_type=MESH)

    def x_copy(step, g_from):
        return pltpu.make_async_remote_copy(
            src_ref=x_all.at[g_from], dst_ref=x_all.at[g_from], send_sem=x_ss.at[step - 1],
            recv_sem=x_rs.at[g_from], device_id=member((me + step) % G), device_id_type=MESH)

    def p_copy(step, block, g_from):
        g_to = (me + step) % G
        return pltpu.make_async_remote_copy(
            src_ref=partial.at[block, g_to], dst_ref=got.at[block, g_from], send_sem=p_ss.at[block, step - 1],
            recv_sem=p_rs.at[block, g_from], device_id=member(g_to), device_id_type=MESH)

    for kind in (POOL, GU, DN):
        own_copy(kind).start()
    halo_copy().start()
    for kind in (POOL, GU, DN):
        for step in range(1, Y):
            y_copy(kind, step).start()
    chain_plane(POOL)
    for s in range(1, Z):
        chain_step(POOL, s)
    chain_plane(GU)
    for step in range(1, S):
        share_copy(step, q).start()

    halo_copy().wait_recv()
    before = rms_scale(halo[...].astype(f32), gain_in[...]).astype(bf16).astype(f32)
    normed[pl.ds(0, margin), :] = jnp.where(t > 0, before, 0.0)
    normed[pl.ds(margin, rows), :] = rms_scale(tokens[...].astype(f32), gain_in[...]).astype(bf16).astype(f32)
    where = t * rows + lax.broadcasted_iota(jnp.int32, (rows, gc), 0)
    for step in range(1, S):
        share_copy(step, (q + step) % S).wait_recv()
    for group, span in enumerate(pool_spans):
        total = normed[:, group * gc : (group + 1) * gc]
        block = total[margin:]
        reach = 1
        while reach < span:
            total = total + pltpu.roll(total, reach, 0)
            reach *= 2
        gap = (total[margin:] / jnp.minimum(where + 1, span).astype(f32) - block).astype(bf16)
        mixed = jnp.dot(gap, pool_all[group], preferred_element_type=f32)
        after[:, group * gc : (group + 1) * gc] = mixed.astype(bf16).astype(f32)
    after[...] = tokens[...].astype(f32) + rms_scale(after[...], gain_out[...])
    whole = rms_scale(after[...], gain_ffn[...]).astype(bf16)
    for k in range(F):
        x_all[me, k] = whole[:, k * depth : (k + 1) * depth]
    for step in range(1, G):
        x_copy(step, me).start()

    acc_g[...] = jnp.zeros_like(acc_g)
    acc_u[...] = jnp.zeros_like(acc_u)

    def times(lhs, rhs):
        return lax.dot_general(lhs, rhs, (((1,), (1,)), ((), ())), preferred_element_type=f32)

    def gate_up(origin):
        def body(g, carry):
            x = x_all[g, origin]
            at = pl.ds(pl.multiple_of(8 + g * rows, 8), rows)
            acc_g[at, :] += times(x, w_gu[origin, 0])
            acc_u[at, :] += times(x, w_gu[origin, 1])
            return carry
        lax.fori_loop(0, G, body, 0)

    chain_step(GU, 1)
    chain_plane(DN)
    for step in range(1, G):
        x_copy(step, (me + step) % G).wait_recv()
    use_plane(gate_up)
    use_step(1, gate_up)
    for s in range(2, Z):
        chain_step(GU, s, gate_up)
    chain_step(DN, 1)

    taps = gate_taps.shape[0]

    def convolve(acc, taps_ref, g, keep):
        block = acc[pl.ds(pl.multiple_of(g * rows, 8), rows + 8), :]
        total = taps_ref[taps - 1 : taps, :] * block[8:]
        for back in range(1, taps):
            moved = pltpu.roll(block, back, 0)[8:]
            total = total + taps_ref[taps - 1 - back : taps - back, :] * jnp.where(keep >= back, moved, 0.0)
        return total

    def activate(g, carry):
        keep = (g % T) * rows + lax.broadcasted_iota(jnp.int32, (rows, cols), 0)
        hidden[g] = (gelu(convolve(acc_g, gate_taps, g, keep)) * convolve(acc_u, up_taps, g, keep)).astype(bf16)
        return carry

    lax.fori_loop(0, G, activate, 0)

    def down(block):
        def body(g, carry):
            partial[block, g] = jnp.dot(hidden[g], w_d[block], preferred_element_type=f32).astype(bf16)
            return carry
        lax.fori_loop(0, G, body, 0)
        for step in range(1, G):
            p_copy(step, block, me).start()
        got[block, me] = partial[block, me]

    use_plane(down)
    use_step(1, down)
    for s in range(2, Z):
        chain_step(DN, s, down)

    def finish(block, carry):
        for step in range(1, G):
            p_copy(step, block, (me + step) % G).wait_recv()
        return carry

    lax.fori_loop(0, F, finish, 0)
    for k in range(F):
        total = got[k, 0].astype(f32)
        for g in range(1, G):
            total = total + got[k, g].astype(f32)
        normed[pl.ds(0, rows), k * depth : (k + 1) * depth] = total
    out[...] = (after[...] + rms_scale(normed[pl.ds(0, rows), :], gain_last[...])).astype(bf16)

    halo_copy().wait_send()
    for step in range(1, S):
        share_copy(step, q).wait_send()
    for step in range(1, G):
        x_copy(step, me).wait_send()
    for kind in (POOL, GU, DN):
        for step in range(1, Y):
            y_copy(kind, step).wait_send()

        def ended(origin, carry):
            @pl.when((origin // Y <= z) & (z + 1 < Z))
            def _():
                chain_copy(kind, origin, 1).wait_send()

            @pl.when((origin // Y >= z) & (z > 0))
            def _():
                chain_copy(kind, origin, -1).wait_send()
            return carry
        lax.fori_loop(0, F, ended, 0)

    def sent(block, carry):
        for step in range(1, G):
            p_copy(step, block, me).wait_send()
        return carry
    lax.fori_loop(0, F, sent, 0)


def solution(mesh):
    def shards(tokens, gain_in, pool, gain_out, gain_ffn, gate_w, up_w, gate_taps, up_taps, down_w, gain_last):
        rows, width = tokens.shape
        depth, columns = gate_w.shape
        plan = Plan(mesh, depth, width, columns)
        F, G, T, Y, Z, cols = plan.F, plan.G, plan.T, plan.Y, plan.Z, plan.cols
        groups, gc = pool.shape[0], pool.shape[2]
        w = jnp.stack([gate_w.T, up_w.T, down_w])
        first = lax.axis_index("tp") * columns
        if plan.joined:
            first = first + (lax.axis_index("rep") * Y + lax.axis_index("fs") % Y) * cols
        gt = lax.dynamic_slice_in_dim(gate_taps, first, cols, 1)
        ut = lax.dynamic_slice_in_dim(up_taps, first, cols, 1)
        margin = max(pool_spans)
        vmem = pl.BlockSpec(memory_space=pltpu.VMEM)
        anywhere = pl.BlockSpec(memory_space=pl.ANY)
        dma = pltpu.SemaphoreType.DMA
        S = min(T, groups)
        V = pltpu.VMEM
        return pl.pallas_call(
            functools.partial(kernel, plan),
            out_shape=jax.ShapeDtypeStruct((rows, width), bf16),
            in_specs=[vmem, vmem, anywhere, vmem, vmem, anywhere, vmem, vmem, vmem],
            out_specs=vmem,
            scratch_shapes=[
                V((margin, width), bf16), V((groups, gc, gc), bf16), V((F, 2, cols, depth), bf16), V((F, cols, depth), bf16),
                V((G, F, rows, depth), bf16), V((margin + rows, width), f32), V((rows, width), f32),
                V((8 + G * rows, cols), f32), V((8 + G * rows, cols), f32), V((G, rows, cols), bf16),
                V((F, G, rows, depth), bf16), V((F, G, rows, depth), bf16),
                dma((3,)), dma((2,)), dma((3, max(Y - 1, 1))), dma((3, F)), dma((3, F)), dma((3, F)),
                dma((max(S - 1, 1),)), dma((S,)), dma((G - 1,)), dma((G,)), dma((F, G - 1)), dma((F, G)),
            ],
            compiler_params=pltpu.CompilerParams(has_side_effects=True, vmem_limit_bytes=61 * 2**20),
            name="layer",
        )(tokens, gain_in[None], pool, gain_out[None], gain_ffn[None], w, gt, ut, gain_last[None])

    in_specs = (
        P(("rep", "fs", "tp"), None), P(), P(None, "fs", None), P(), P(),
        P("fs", "tp"), P("fs", "tp"), P(), P(), P("tp", "fs"), P(),
    )
    return jax.shard_map(shards, mesh=mesh, in_specs=in_specs, out_specs=P(("rep", "fs", "tp"), None), check_vma=False)
```

time: 601 us -> 224 us (0.37)
  waiting for transfers between devices: 533 us -> 0 us
  Pallas kernels: 0 us -> 212 us
  matrix products: 39.9 us -> 0 us
  between operations: 13.6 us -> 0.03 us
  other arithmetic: 11.2 us -> 3.38 us
    all_gather x5 -> x0, waiting for transfers between devices: 523 us -> none  [the longest x1 159 us: shards(): lax.all_gather(gate_weight, 'fs', axis=0, tiled=True)]
    pallas_call x0 -> x1, Pallas kernels: none -> 212 us  [shards(): pl.pallas_call(functools.partial(kernel, plan), out_shape=jax.ShapeDtypeS...]
    dot_general x4 -> x0, matrix products: 39.9 us -> none  [the longest x1 18 us: shards(): jnp.dot(hidden, down_full, preferred_element_type=jnp.float32)]
    reduce_scatter x1 -> x0, waiting for transfers between devices: 7.37 us -> none  [shards(): lax.psum_scatter(jnp.dot(hidden, down_full, preferred_element_type=jnp.fl...]
  transfers between devices with their start and end apart: 6 -> 0, of which waited for: 6 -> 0; matrix products, arithmetic and copies ran while one was open for 5% -> 0% of each run, Pallas kernels for 0% -> 0%
where the time goes in v1:
time: 224 us; the launch traced here: 222 us
  Pallas kernels  212 us (95%)
  local copies, waits for them, and re-layouts  6.86 us (3%)
  other arithmetic  3.38 us (2%)
    pallas_call x1, Pallas kernels, shards(): pl.pallas_call(functools.partial(kernel, plan), out_shape=jax.ShapeDtypeS...  212 us
    unnamed x3, local copies, waits for them, and re-layouts  5.45 us

profile of v1, /device:TPU:0, one launch (start us, length us, event | category | flops | bytes accessed | tf_op | source)
XLA Modules:
  0.0 222.0 jit_solution(10163081823646439284)
XLA Ops:
  0.0 1.7 copy.13
  1.7 1.7 copy.12
  3.4 3.4 %pad_maximum_fusion.w = bf16[3,2816,256]{2,1,0:T(8,128)(2,1)} fusion(bf16[1,2816,256]{2,1,0:T(8,128)(2,1)} %bitcast.13, bf16[1,2816,256]{2,1,0:T(8,128)(2,1)S(1)} %bitcast.11, bf16[1,2816,256]{2,1,0:T(8,128)(2,1)S(1)} %bitcast.12), kind=kLoop, calls=%fused_computation | loop fusion | flops 4325376 | bytes 8650752 | tf_op jit(solution)/shard_map/stack | solution.py:317
  6.8 1.4 constant_dynamic-slice_fusion
  8.2 211.7 %layer.1 = bf16[192,2048]{1,0:T(8,128)(2,1)} custom-call(bf16[192,2048]{1,0:T(8,128)(2,1)} %tokens.1, f32[1,2048]{1,0:T(1,128)} %bitcast.14, bf16[4,64,512]{2,1,0:T(8,128)(2,1)} %pool.1, f32[1,2048]{1,0:T(1,128)} %bitcast.15, f32[1,2048]{1,0:T(1,128)} %bitcast.16, bf16[3,2816,256]{2,1,0:T(8,128)(2,1)} %pad_maximum_fusion.w, ...), custom_call_target="tpu_custom_call" | custom-call | tf_op jit(solution)/shard_map/layer/pallas_call | solution.py:329
  219.9 2.1 copy.15

commit v2 on v1

--- a/solution.py
+++ b/solution.py
@@ -39,9 +39,9 @@
 
 
 def kernel(
-    plan, tokens, gain_in, pool, gain_out, gain_ffn, w, gate_taps, up_taps, gain_last, out,
-    halo, pool_all, w_gu, w_d, x_all, normed, after, acc_g, acc_u, hidden, partial, got,
-    own_sem, halo_sem, y_ss, up_ss, dn_ss, piece_rs, share_ss, share_rs, x_ss, x_rs, p_ss, p_rs,
+    plan, tokens, gain_in, pool, gain_out, gain_ffn, gate_t, up_t, down_w, gate_taps, up_taps, gain_last, out,
+    halo, pool_all, w_gu, w_d, x_all, normed, after, acc_g, acc_u, hidden, partial, swapped, summed, got,
+    own_sem, halo_sem, y_ss, up_ss, dn_ss, piece_rs, share_ss, share_rs, x_ss, x_rs, f_ss, s_ss, s_rs, p_ss, p_rs,
 ):
     R, F, T, Y, Z, G, cols = plan.R, plan.F, plan.T, plan.Y, plan.Z, plan.G, plan.cols
     r, f, t = lax.axis_index("rep"), lax.axis_index("fs"), lax.axis_index("tp")
@@ -54,17 +54,17 @@
     GS = groups // S
     q = t % S
     margin = halo.shape[0]
-    POOL, GU, DN = 0, 1, 2
-
-    if plan.joined:
-        me = (r * Y + y) * T + t
-    else:
-        me = t
-
-    def member(g):
-        if plan.joined:
-            return {"rep": g // (T * Y), "fs": z * Y + (g // T) % Y, "tp": g % T}
-        return {"tp": g}
+    C = G // T
+    POOL, GA, UP, DN = 0, 1, 2, 3
+    kinds = (POOL, GA, UP, DN)
+    GU = (GA, UP)
+
+    chip = r * Y + y if plan.joined else 0
+    me = chip * T + t
+
+    def peer(step):
+        to = (chip + step) % C
+        return {"rep": to // Y, "fs": z * Y + to % Y}
 
     def sub_of(y_to):
         return r * Y + y_to if plan.joined else 0
@@ -75,14 +75,12 @@
     def slot(kind, origin):
         if kind == POOL:
             return pool_all.at[pl.ds(q * GS, GS), pl.ds(pl.multiple_of(origin * slab, slab), slab)]
-        return w_gu.at[origin] if kind == GU else w_d.at[origin]
+        return w_d.at[origin] if kind == DN else w_gu.at[origin, kind - GA]
 
     def source(kind, y_to):
         if kind == POOL:
             return pool.at[pl.ds(q * GS, GS)]
-        if kind == GU:
-            return w.at[pl.ds(0, 2), w_rows(y_to)]
-        return w.at[2, w_rows(y_to)]
+        return (gate_t, up_t, down_w)[kind - GA].at[w_rows(y_to)]
 
     def own_copy(kind):
         return pltpu.make_async_copy(source(kind, y), slot(kind, f), own_sem.at[kind])
@@ -98,59 +96,43 @@
             src_ref=slot(kind, origin), dst_ref=slot(kind, origin), send_sem=(up_ss if dz > 0 else dn_ss).at[kind, origin],
             recv_sem=piece_rs.at[kind, origin], device_id={"fs": (z + dz) * Y + y}, device_id_type=MESH)
 
-    def send_up(kind, origin):
-        @pl.when(z + 1 < Z)
-        def _():
-            chain_copy(kind, origin, 1).start()
-
-    def send_down(kind, origin):
-        @pl.when(z > 0)
-        def _():
-            chain_copy(kind, origin, -1).start()
-
     def arrived(kind, origin):
         chain_copy(kind, origin, 1).wait_recv()
 
-    def chain_plane(kind):
-        own_copy(kind).wait()
-        send_up(kind, f)
-        send_down(kind, f)
-        for step in range(1, Y):
-            origin = z * Y + (y + step) % Y
+    def pass_on(kind, origin, z0):
+        @pl.when((z0 <= z) & (z + 1 < Z))
+        def _():
+            chain_copy(kind, origin, 1).start()
+
+        @pl.when((z0 >= z) & (z > 0))
+        def _():
+            chain_copy(kind, origin, -1).start()
+
+    side = jnp.minimum(z, Z - 1 - z)
+
+    def place(k):
+        j = k // Y
+        near = jnp.where(j % 2 == 1, z - (j + 1) // 2, z + j // 2)
+        far = jnp.where(2 * z <= Z - 1, j, Z - 1 - j)
+        z0 = jnp.where(j <= 2 * side, near, far)
+        return z0, z0 * Y + (y + k % Y) % Y
+
+    def chain(kinds_now, k):
+        z0, origin = place(k)
+        for kind in kinds_now:
             arrived(kind, origin)
-            send_up(kind, origin)
-            send_down(kind, origin)
-
-    def chain_step(kind, s, use=None):
-        for step in range(Y):
-            @pl.when(z >= s)
-            def _():
-                origin = (z - s) * Y + (y + step) % Y
-                arrived(kind, origin)
-                send_up(kind, origin)
-
-            @pl.when(z + s < Z)
-            def _():
-                origin = (z + s) * Y + (y + step) % Y
-                arrived(kind, origin)
-                send_down(kind, origin)
-        if use is not None:
-            use_step(s, use)
-
-    def use_step(s, use):
-        for sign in (-1, 1):
-            @pl.when((z >= s) if sign < 0 else (z + s < Z))
-            def _():
-                def body(step, carry):
-                    use((z + sign * s) * Y + (y + step) % Y)
-                    return carry
-                lax.fori_loop(0, Y, body, 0)
-
-    def use_plane(use):
-        def body(step, carry):
-            use(z * Y + (y + step) % Y)
-            return carry
-        lax.fori_loop(0, Y, body, 0)
+            pass_on(kind, origin, z0)
+
+    def chain_own(kinds_now):
+        for kind in kinds_now:
+            own_copy(kind).wait()
+            pass_on(kind, f, z)
+
+    def chain_range(kinds_now, first, last):
+        def body(k, carry):
+            chain(kinds_now, k)
+            return carry
+        lax.fori_loop(first, last, body, 0)
 
     def halo_copy():
         return pltpu.make_async_remote_copy(
@@ -163,27 +145,39 @@
             send_sem=share_ss.at[step - 1], recv_sem=share_rs.at[q_from],
             device_id={"tp": t - q + (q + step) % S}, device_id_type=MESH)
 
-    def x_copy(step, g_from):
-        return pltpu.make_async_remote_copy(
-            src_ref=x_all.at[g_from], dst_ref=x_all.at[g_from], send_sem=x_ss.at[step - 1],
-            recv_sem=x_rs.at[g_from], device_id=member((me + step) % G), device_id_type=MESH)
-
-    def p_copy(step, block, g_from):
-        g_to = (me + step) % G
-        return pltpu.make_async_remote_copy(
-            src_ref=partial.at[block, g_to], dst_ref=got.at[block, g_from], send_sem=p_ss.at[block, step - 1],
-            recv_sem=p_rs.at[block, g_from], device_id=member(g_to), device_id_type=MESH)
-
-    for kind in (POOL, GU, DN):
+    def x_copy(step, c_from):
+        g = c_from * T + t
+        return pltpu.make_async_remote_copy(
+            src_ref=x_all.at[g], dst_ref=x_all.at[g], send_sem=x_ss.at[step - 1],
+            recv_sem=x_rs.at[g], device_id=peer(step), device_id_type=MESH)
+
+    def x_across(step, c, t_from):
+        g = c * T + t_from
+        return pltpu.make_async_remote_copy(
+            src_ref=x_all.at[g], dst_ref=x_all.at[g], send_sem=f_ss.at[step - 1, c],
+            recv_sem=x_rs.at[g], device_id={"tp": (t + step) % T}, device_id_type=MESH)
+
+    def s_copy(step, block, t_from):
+        t_to = (t + step) % T
+        return pltpu.make_async_remote_copy(
+            src_ref=partial.at[block, t_to], dst_ref=swapped.at[block, t_from], send_sem=s_ss.at[block, step - 1],
+            recv_sem=s_rs.at[block, t_from], device_id={"tp": t_to}, device_id_type=MESH)
+
+    def p_copy(step, block, c_from):
+        return pltpu.make_async_remote_copy(
+            src_ref=summed.at[block, (chip + step) % C], dst_ref=got.at[block, c_from], send_sem=p_ss.at[block, step - 1],
+            recv_sem=p_rs.at[block, c_from], device_id=peer(step), device_id_type=MESH)
+
+    for kind in kinds:
         own_copy(kind).start()
     halo_copy().start()
-    for kind in (POOL, GU, DN):
+    for kind in kinds:
         for step in range(1, Y):
             y_copy(kind, step).start()
-    chain_plane(POOL)
-    for s in range(1, Z):
-        chain_step(POOL, s)
-    chain_plane(GU)
+    chain_own((POOL,))
+    chain_own(GU)
+    chain_range((POOL,), 1, F)
+    chain_range(GU, 1, Y)
     for step in range(1, S):
         share_copy(step, q).start()
 
@@ -208,8 +202,10 @@
     whole = rms_scale(after[...], gain_ffn[...]).astype(bf16)
     for k in range(F):
         x_all[me, k] = whole[:, k * depth : (k + 1) * depth]
-    for step in range(1, G):
-        x_copy(step, me).start()
+    for step in range(1, C):
+        x_copy(step, chip).start()
+    for step in range(1, T):
+        x_across(step, chip, t).start()
 
     acc_g[...] = jnp.zeros_like(acc_g)
     acc_u[...] = jnp.zeros_like(acc_u)
@@ -226,15 +222,27 @@
             return carry
         lax.fori_loop(0, G, body, 0)
 
-    chain_step(GU, 1)
-    chain_plane(DN)
-    for step in range(1, G):
-        x_copy(step, (me + step) % G).wait_recv()
-    use_plane(gate_up)
-    use_step(1, gate_up)
-    for s in range(2, Z):
-        chain_step(GU, s, gate_up)
-    chain_step(DN, 1)
+    ahead = Y * (1 + jnp.maximum(1, 2 * side))
+    chain_range(GU, Y, ahead)
+    chain_own((DN,))
+    chain_range((DN,), 1, Y)
+    for back in range(1, C):
+        c = (chip + C - back) % C
+        x_copy(back, c).wait_recv()
+        for step in range(1, T):
+            x_across(step, c, t).start()
+    for c in range(C):
+        for step in range(1, T):
+            x_across(step, c, (t + step) % T).wait_recv()
+
+    def gate_up_step(k, carry):
+        @pl.when(k >= ahead)
+        def _():
+            chain(GU, k)
+        gate_up(place(k)[1])
+        return carry
+    lax.fori_loop(0, F, gate_up_step, 0)
+    chain_range((DN,), Y, ahead)
 
     taps = gate_taps.shape[0]
 
@@ -254,38 +262,67 @@
     lax.fori_loop(0, G, activate, 0)
 
     def down(block):
-        def body(g, carry):
-            partial[block, g] = jnp.dot(hidden[g], w_d[block], preferred_element_type=f32).astype(bf16)
-            return carry
-        lax.fori_loop(0, G, body, 0)
-        for step in range(1, G):
-            p_copy(step, block, me).start()
-        got[block, me] = partial[block, me]
-
-    use_plane(down)
-    use_step(1, down)
-    for s in range(2, Z):
-        chain_step(DN, s, down)
+        def body(i, carry):
+            step, c = i // C + 1, i % C
+            t_to = (t + step) % T
+            product = jnp.dot(hidden[c * T + t_to], w_d[block], preferred_element_type=f32)
+            partial[block, t_to, c] = product.astype(bf16)
+            return carry
+        lax.fori_loop(0, G - C, body, 0)
+        for step in range(1, T):
+            s_copy(step, block, t).start()
+        lax.fori_loop(G - C, G, body, 0)
+
+    def add_up(block):
+        for back in range(1, T):
+            s_copy(back, block, (t + back) % T).wait_recv()
+
+        def body(c, carry):
+            total = partial[block, t, c].astype(f32)
+            for back in range(1, T):
+                total = total + swapped[block, (t + back) % T, c].astype(f32)
+            summed[block, c] = total.astype(bf16)
+            return carry
+        lax.fori_loop(0, C, body, 0)
+        for step in range(1, C):
+            p_copy(step, block, chip).start()
+        got[block, chip] = summed[block, chip]
+
+    def down_step(k, carry):
+        @pl.when(k >= ahead)
+        def _():
+            chain((DN,), k)
+        down(place(k)[1])
+
+        @pl.when(k > 0)
+        def _():
+            add_up(place(k - 1)[1])
+        return carry
+    lax.fori_loop(0, F, down_step, 0)
+    add_up(place(F - 1)[1])
 
     def finish(block, carry):
-        for step in range(1, G):
-            p_copy(step, block, (me + step) % G).wait_recv()
+        for step in range(1, C):
+            p_copy(step, block, (chip + step) % C).wait_recv()
         return carry
 
     lax.fori_loop(0, F, finish, 0)
     for k in range(F):
         total = got[k, 0].astype(f32)
-        for g in range(1, G):
-            total = total + got[k, g].astype(f32)
+        for c in range(1, C):
+            total = total + got[k, c].astype(f32)
         normed[pl.ds(0, rows), k * depth : (k + 1) * depth] = total
     out[...] = (after[...] + rms_scale(normed[pl.ds(0, rows), :], gain_last[...])).astype(bf16)
 
     halo_copy().wait_send()
     for step in range(1, S):
         share_copy(step, q).wait_send()
-    for step in range(1, G):
-        x_copy(step, me).wait_send()
-    for kind in (POOL, GU, DN):
+    for step in range(1, C):
+        x_copy(step, chip).wait_send()
+    for step in range(1, T):
+        for c in range(C):
+            x_across(step, c, t).wait_send()
+    for kind in kinds:
         for step in range(1, Y):
             y_copy(kind, step).wait_send()
 
@@ -301,8 +338,10 @@
         lax.fori_loop(0, F, ended, 0)
 
     def sent(block, carry):
-        for step in range(1, G):
-            p_copy(step, block, me).wait_send()
+        for step in range(1, T):
+            s_copy(step, block, t).wait_send()
+        for step in range(1, C):
+            p_copy(step, block, chip).wait_send()
         return carry
     lax.fori_loop(0, F, sent, 0)
 
@@ -314,7 +353,7 @@
         plan = Plan(mesh, depth, width, columns)
         F, G, T, Y, Z, cols = plan.F, plan.G, plan.T, plan.Y, plan.Z, plan.cols
         groups, gc = pool.shape[0], pool.shape[2]
-        w = jnp.stack([gate_w.T, up_w.T, down_w])
+        C = G // T
         first = lax.axis_index("tp") * columns
         if plan.joined:
             first = first + (lax.axis_index("rep") * Y + lax.axis_index("fs") % Y) * cols
@@ -329,19 +368,20 @@
         return pl.pallas_call(
             functools.partial(kernel, plan),
             out_shape=jax.ShapeDtypeStruct((rows, width), bf16),
-            in_specs=[vmem, vmem, anywhere, vmem, vmem, anywhere, vmem, vmem, vmem],
+            in_specs=[vmem, vmem, anywhere, vmem, vmem, anywhere, anywhere, anywhere, vmem, vmem, vmem],
             out_specs=vmem,
             scratch_shapes=[
                 V((margin, width), bf16), V((groups, gc, gc), bf16), V((F, 2, cols, depth), bf16), V((F, cols, depth), bf16),
                 V((G, F, rows, depth), bf16), V((margin + rows, width), f32), V((rows, width), f32),
                 V((8 + G * rows, cols), f32), V((8 + G * rows, cols), f32), V((G, rows, cols), bf16),
-                V((F, G, rows, depth), bf16), V((F, G, rows, depth), bf16),
-                dma((3,)), dma((2,)), dma((3, max(Y - 1, 1))), dma((3, F)), dma((3, F)), dma((3, F)),
-                dma((max(S - 1, 1),)), dma((S,)), dma((G - 1,)), dma((G,)), dma((F, G - 1)), dma((F, G)),
+                V((F, T, C, rows, depth), bf16), V((F, T, C, rows, depth), bf16), V((F, C, rows, depth), bf16), V((F, C, rows, depth), bf16),
+                dma((4,)), dma((2,)), dma((4, max(Y - 1, 1))), dma((4, F)), dma((4, F)), dma((4, F)),
+                dma((max(S - 1, 1),)), dma((S,)), dma((max(C - 1, 1),)), dma((G,)),
+                dma((max(T - 1, 1), C)), dma((F, max(T - 1, 1))), dma((F, T)), dma((F, max(C - 1, 1))), dma((F, C)),
             ],
             compiler_params=pltpu.CompilerParams(has_side_effects=True, vmem_limit_bytes=61 * 2**20),
             name="layer",
-        )(tokens, gain_in[None], pool, gain_out[None], gain_ffn[None], w, gt, ut, gain_last[None])
+        )(tokens, gain_in[None], pool, gain_out[None], gain_ffn[None], gate_w.T, up_w.T, down_w, gt, ut, gain_last[None])
 
     in_specs = (
         P(("rep", "fs", "tp"), None), P(), P(None, "fs", None), P(), P(),

time: 224 us -> 201 us (0.90)
  Pallas kernels: 212 us -> 193 us
  other arithmetic: 3.38 us -> 0 us
    pallas_call x1, Pallas kernels: 212 us -> 193 us  [shards(): pl.pallas_call(functools.partial(kernel, plan), out_shape=jax.ShapeDtypeS...]
    another operation x1 -> x0, other arithmetic: 3.38 us -> none  [shards(): w = jnp.stack([gate_w.T, up_w.T, down_w])]
    unnamed x3 -> x5, local copies, waits for them, and re-layouts: 5.45 us -> 6.31 us
where the time goes in v2:
time: 201 us
  Pallas kernels  193 us (96%)
  local copies, waits for them, and re-layouts  7.72 us (4%)
    pallas_call x1, Pallas kernels, shards(): pl.pallas_call(functools.partial(kernel, plan), out_shape=jax.ShapeDtypeS...  193 us
    unnamed x5, local copies, waits for them, and re-layouts  6.31 us

profile of v2, /device:TPU:0, one launch (start us, length us, event | category | flops | bytes accessed | tf_op | source)
XLA Modules:
  0.0 200.8 jit_solution(1656154453861352337)
XLA Ops:
  0.0 1.4 constant_dynamic-slice_fusion
  1.4 0.0 copy-start
  1.4 2.6 %copy.12 = bf16[256,2816]{0,1:T(8,128)(2,1)} copy(bf16[256,2816]{1,0:T(8,128)(2,1)} %param.16) | data formatting | bytes 2883584 | tf_op args[5]
  4.1 0.0 copy-done
  4.1 1.6 copy.13
  5.6 193.0 %layer.1 = bf16[192,2048]{1,0:T(8,128)(2,1)} custom-call(bf16[192,2048]{1,0:T(8,128)(2,1)} %tokens.1, f32[1,2048]{1,0:T(1,128)} %bitcast.8, bf16[4,64,512]{2,1,0:T(8,128)(2,1)} %pool.1, f32[1,2048]{1,0:T(1,128)} %bitcast.9, f32[1,2048]{1,0:T(1,128)} %bitcast.10, bf16[2816,256]{1,0:T(8,128)(2,1)} %bitcast.6, bf16[2816,256]{1,0:T(8,128)(2,1)} %bitcast.7, ...), custom_call_target="tpu_custom_call" | custom-call | tf_op jit(solution)/shard_map/layer/pallas_call | solution.py:368
  198.7 2.1 %copy.15 = bf16[192,2048]{1,0:T(8,128)(2,1)} copy(bf16[192,2048]{1,0:T(8,128)(2,1)} %layer.1) | data formatting | bytes 1572864
Async XLA Ops:
  1.4 2.7 %copy-start = (bf16[256,2816]{1,0:T(8,128)(2,1)S(1)}, bf16[256,2816]{1,0:T(8,128)(2,1)}, u32[]{:S(2)}) copy-start(bf16[256,2816]{1,0:T(8,128)(2,1)} %param.17) | copy-start | bytes 4325380
